TPU v7x, 128 devices: a whole 4x4x4 slice. The times are simulated.
128 devices in a mesh: fs: 16 (over z, y), tp: 8 (over x, core).
Axes of the slice: x: 4, y: 4, z: 4, core: 2. Of those that a mesh axis runs over, the one named last changes fastest.
Arguments:
- tokens: bfloat16 [16384, 2048], P('fs', 'tp'), may hold values from -6 to 6
- norm_gain: float32 [2048], P('fs'), may hold values from 0.1 to 1.9
- up_master: float32 [2048, 8192], P('fs', 'tp'), may hold values from -0.125 to 0.125
- down_master: float32 [2048, 8192], P('fs', 'tp'), may hold values from -0.0625 to 0.0625
Outputs:
- up_weights: bfloat16 [2048, 8192], P(None, 'tp')
- down_weights: bfloat16 [8192, 2048], P('tp')
- mlp_out: bfloat16 [16384, 2048], P('fs', 'tp')
All inputs are finite; a program needn't handle non-finite values.
Results may differ from a plain program's by a relative error of at most 0.014.
Values may be sent and summed in bfloat16 or wider, within the bound.
A program may use at most 128 MiB of HBM per device.

v0:
```python
import jax
import jax.numpy as jnp
from jax import lax
from jax.sharding import PartitionSpec as P

norm_floor = 1e-06


def side_by_side(arrays, axis, dim, along):
    ends, at = ([], 0)
    for a in arrays[:-1]:
        at += a.shape[along]
        ends.append(at)
    both = jnp.concatenate(arrays, axis=along)
    return tuple(jnp.split(lax.all_gather(both, axis, axis=dim, tiled=True), ends, axis=along))


def on_device(tokens, norm_gain, up_master, down_master):
    up_local = (norm_gain[:, None] * up_master).astype(jnp.bfloat16)
    down_local = down_master.astype(jnp.bfloat16)
    gathered = lax.all_gather(tokens, "tp", axis=1, tiled=True)
    widened = gathered.astype(jnp.float32)
    normed = (
        widened * lax.rsqrt(jnp.mean(widened * widened, axis=-1, keepdims=True) + norm_floor)
    ).astype(jnp.bfloat16)
    up_whole, down_whole = side_by_side((up_local, down_local), "fs", 0, 1)
    preact = jnp.dot(normed, up_whole, preferred_element_type=jnp.float32)
    hidden = jnp.square(jax.nn.relu(preact)).astype(jnp.bfloat16)
    partial_value = jnp.einsum("tf,df->td", hidden, down_whole, preferred_element_type=jnp.float32)
    summed = lax.psum_scatter(
        partial_value.astype(jnp.bfloat16), "tp", scatter_dimension=1, tiled=True
    )
    return (up_whole, jnp.transpose(down_whole), summed)


def solution(mesh):
    in_specs = (P("fs", "tp"), P("fs"), P("fs", "tp"), P("fs", "tp"))
    out_specs = (P(None, "tp"), P("tp", None), P("fs", "tp"))
    return jax.shard_map(
        on_device, mesh=mesh, in_specs=in_specs, out_specs=out_specs, check_vma=False
    )
```

profile of v0, /device:TPU:0, one launch (start us, length us, event | category | flops | bytes accessed | tf_op | source)
XLA Modules:
  0.0 186.4 jit_solution(12943971067631530127)
XLA Ops:
  7.2 0.0 all-gather.5.cloned.1.call-start
  7.2 0.7 all-gather.5.cloned.1.call-update
  7.9 0.0 all-gather.3.cloned.1.call-start
  7.9 1.2 copy.7
  9.2 1.2 copy.8
  10.4 0.7 multiply_convert_fusion.2
  11.1 0.8 pad_maximum_fusion
  11.9 0.0 all-gather.3.cloned.1.call-update
  12.0 0.0 reduce-scatter.2.cloned.1.call-start
  12.0 35.6 %all-gather.5.cloned.1.call-done = bf16[1024,2048]{1,0:T(8,128)(2,1)} async-done(((bf16[1024,256]{1,0:T(8,128)(2,1)}), bf16[1024,2048]{1,0:T(8,128)(2,1)}) %all-gather.5.cloned.1.call-update) | async-done | bytes 4194320 | tf_op jit(solution)/shard_map/all_gather | solution.py:21
  47.7 3.1 %fusion = f32[1024]{0:T(1024)S(1)} fusion(bf16[1024,2048]{1,0:T(8,128)(2,1)} %all-gather.5.cloned.1.call-done), kind=kLoop, calls=%fused_computation.2 | loop fusion | flops 6290432 | bytes 4198400 | tf_op jit(solution)/shard_map/reduce_sum | solution.py:24
  50.7 78.0 %all-gather.3.cloned.1.call-done = bf16[2048,2048]{0,1:T(8,128)(2,1)} async-done(((bf16[128,2048]{0,1:T(8,128)(2,1)}), bf16[2048,2048]{0,1:T(8,128)(2,1)}) %all-gather.3.cloned.1.call-update) | async-done | bytes 8388624 | tf_op jit(solution)/shard_map/all_gather | solution.py:15
  128.7 0.0 copy-start
  128.7 7.7 %fusion.2 = f32[1024,1024]{1,0:T(8,128)S(1)} fusion(bf16[1024,2048]{1,0:T(8,128)(2,1)} %all-gather.5.cloned.1.call-done, f32[1024]{0:T(1024)S(1)} %add_rsqrt_fusion, bf16[2048,2048]{0,1:T(8,128)(2,1)} %all-gather.3.cloned.1.call-done), kind=kOutput, calls=%fused_computation.4 | convolution fusion | flops 4301258752 | bytes 12587008 | tf_op jit(solution)/shard_map/dot_general | solution.py:27
  136.5 0.0 copy-done
  136.5 6.1 %convolution_convert_fusion = bf16[1024,2048]{1,0:T(8,128)(2,1)} fusion(bf16[2048,2048]{0,1:T(8,128)(2,1)S(1)} %copy-done, f32[1024,1024]{1,0:T(8,128)S(1)} %fusion.2), kind=kOutput, calls=%fused_computation.7 | convolution fusion | flops 4300210176 | bytes 12582912 | tf_op jit(solution)/shard_map/tf,df->td/dot_general | solution.py:29
  142.6 0.0 reduce-scatter.2.cloned.1.call-update
  142.6 6.2 %slice_bitcast_fusion = (bf16[1024,2048]{1,0:T(8,128)(2,1)}, bf16[2048,1024]{0,1:T(8,128)(2,1)}) fusion(bf16[2048,2048]{0,1:T(8,128)(2,1)} %all-gather.3.cloned.1.call-done), kind=kLoop, calls=%fused_computation.9 | loop fusion | bytes 16777216 | tf_op jit(solution)/shard_map/transpose | solution.py:33
  148.7 6.4 %copy.9 = bf16[2048,1024]{1,0:T(8,128)(2,1)} copy(bf16[2048,1024]{0,1:T(8,128)(2,1)} %get-tuple-element.7) | data formatting | bytes 8388608
  155.2 24.7 %reduce-scatter.2.cloned.1.call-done = bf16[1024,256]{1,0:T(8,128)(2,1)} async-done(((bf16[1024,2048]{1,0:T(8,128)(2,1)}), bf16[1024,256]{1,0:T(8,128)(2,1)}) %reduce-scatter.2.cloned.1.call-update) | async-done | bytes 524304 | tf_op jit(solution)/shard_map/reduce_scatter | solution.py:30
  (1 shorter events, 0.0 us)
Async XLA Ops:
  7.2 40.5 %all-gather.5.cloned.1.call-start = ((), (), s32[]{:S(2)}) async-start(), calls=%async_computation.2 | async-start | bytes 4718592 | tf_op jit(solution)/shard_map/all_gather | solution.py:21
  7.9 120.8 %all-gather.3.cloned.1.call-start = ((), (), s32[]{:S(2)}) async-start(), calls=%async_computation.1 | async-start | bytes 8912896 | tf_op jit(solution)/shard_map/all_gather | solution.py:15
  12.0 167.9 %reduce-scatter.2.cloned.1.call-start = ((), (), s32[]{:S(2)}) async-start(), calls=%async_computation.3 | async-start | bytes 4718592 | tf_op jit(solution)/shard_map/reduce_scatter | solution.py:30
  128.7 7.8 %copy-start = (bf16[2048,2048]{0,1:T(8,128)(2,1)S(1)}, bf16[2048,2048]{0,1:T(8,128)(2,1)}, u32[]{:S(2)}) copy-start(bf16[2048,2048]{0,1:T(8,128)(2,1)} %all-gather.3.cloned.1.call-done) | copy-start | bytes 25165828
Sparse Core Ops, SparseCore 0:
  9.7 37.9 all-gather.4
  50.3 78.3 all-gather.2
  142.7 37.0 reduce-scatter.1
where the time goes:
time: 187 us; the launch traced here: 186 us
  waiting for transfers between devices  139 us (74%)
  local copies, waits for them, and re-layouts  15 us (8%)
  matrix products  13.8 us (7%)
  between operations  13.8 us (7%)
  other arithmetic  4.6 us (2%)
    all_gather x1, waiting for transfers between devices, side_by_side(): lax.all_gather(both, axis, axis=dim, tiled=True)  78 us
    all_gather x1, waiting for transfers between devices, on_device(): gathered = lax.all_gather(tokens, 'tp', axis=1, tiled=True)  35.6 us
    reduce_scatter x1, waiting for transfers between devices, on_device(): lax.psum_scatter(partial_value.astype(jnp.bfloat16), 'tp', scatter_dimens...  24.7 us
    unnamed x5, local copies, waits for them, and re-layouts  8.86 us
    dot_general x1, matrix products, on_device(): preact = jnp.dot(normed, up_whole, preferred_element_type=jnp.float32)  7.74 us
    transpose x1, local copies, waits for them, and re-layouts, on_device(): return (up_whole, jnp.transpose(down_whole), summed)  6.15 us
    dot_general x1, matrix products, on_device(): jnp.einsum('tf,df->td', hidden, down_whole, preferred_element_type=jnp.fl...  6.09 us
  transfers between devices with their start and end apart: 3, of which 3 were waited for; matrix products, arithmetic and copies ran while one was open for 11% of the time, Pallas kernels for 0%

commit v1 on v0

v1 whole, which is shorter than its diff:
```python
import jax
import jax.numpy as jnp
from jax import lax
from jax.experimental import pallas as pl
from jax.experimental.pallas import tpu as pltpu
from jax.sharding import PartitionSpec as P

norm_floor = 1e-06

MESH = pl.DeviceIdType.MESH
BF, F32 = jnp.bfloat16, jnp.float32
D, FF = 2048, 8192
ROWS = 1024
TILE = 256
UP, DN = 0, 1


def kernel(
    tok_in, gain_in, up_in, dn_in,
    up_v, dn_v, out_v,
    up32, dn32, gain_v, tok_v, scale_v, hid, pbuf, prx, fwd, qf, fin,
    in_sem, w_send, w_recv, t_send, t_recv, r_send, r_recv,
):
    fs, tp = lax.axis_index("fs"), lax.axis_index("tp")
    z, y, x, c = fs // 4, fs % 4, tp // 2, tp % 2
    mod4 = lambda v: lax.rem(v + 8, 4)
    to_y = lambda s: {"fs": z * 4 + mod4(y + s), "tp": tp}
    to_z = lambda s: {"fs": mod4(z + s) * 4 + y, "tp": tp}
    to_x = lambda s: {"fs": fs, "tp": mod4(x + s) * 2 + c}
    partner = {"fs": fs, "tp": x * 2 + 1 - c}

    loads = [
        pltpu.make_async_copy(up_in, up32, in_sem.at[0]),
        pltpu.make_async_copy(gain_in, gain_v, in_sem.at[1]),
        pltpu.make_async_copy(tok_in, tok_v.at[tp], in_sem.at[2]),
        pltpu.make_async_copy(dn_in, dn32, in_sem.at[3]),
    ]
    for load in loads:
        load.start()
    barrier = pltpu.get_barrier_semaphore()
    for peer in (to_y(1), to_y(-1), to_z(1), to_z(-1), to_x(1), to_x(-1), partner):
        pl.semaphore_signal(barrier, inc=1, device_id=peer, device_id_type=MESH)

    sends = []

    def remote(src, dst, landed, send_sem, recv_sem, peer):
        out = lambda: pltpu.make_async_remote_copy(src, dst, send_sem, recv_sem, peer, MESH)
        back = lambda: pltpu.make_async_remote_copy(landed, landed, send_sem, recv_sem, peer, MESH)
        return out, back

    def go(pair):
        copy = pair[0]()
        copy.start()
        sends.append(copy)

    def weight_copies(w, h):
        first, second = (to_y, to_z) if h == 0 else (to_z, to_y)
        ia, ib = (y, z) if h == 0 else (z, y)

        def piece(da, db, q):
            a, b = mod4(ia + da), mod4(ib + db)
            f = b * 4 + a if h == 0 else a * 4 + b
            if w == UP:
                at, n = f * 128 + (0 if q is None else 64 * q), 128 if q is None else 64
                return up_v.at[h, pl.ds(pl.multiple_of(at, 64), n)]
            at, n = 512 * h + (0 if q is None else 256 * q), 512 if q is None else 256
            return dn_v.at[f, pl.ds(at, n)]

        table, count = {}, [0]

        def add(name, sent, peer, landed):
            k = count[0]
            count[0] += 1
            table[name] = remote(piece(*sent), piece(*sent), piece(*landed), w_send.at[w, h, k], w_recv.at[w, h, k], peer)

        for s, sign in (("+", 1), ("-", -1)):
            q = 0 if sign == 1 else 1
            add("S" + s, (0, 0, None), first(sign), (-sign, 0, None))
            add("F" + s, (-sign, 0, q), first(sign), (2, 0, q))
            for a in (0, -1, 1):
                add((a, "T" + s), (a, 0, None), second(sign), (a, -sign, None))
                add((a, "G" + s), (a, -sign, q), second(sign), (a, 2, q))
            for part in (0, 1):
                add((2, "T" + s, part), (2, 0, part), second(sign), (2, -sign, part))
            add((2, "G" + s), (2, -sign, q), second(sign), (2, 2, q))
        return table

    W = [[weight_copies(w, h) for h in (0, 1)] for w in (UP, DN)]

    def e0(w):
        for h in (0, 1):
            go(W[w][h]["S+"]), go(W[w][h]["S-"])
        for h in (0, 1):
            go(W[w][h][0, "T+"]), go(W[w][h][0, "T-"])

    def e1(w):
        for s, a in (("+", -1), ("-", 1)):
            for h in (0, 1):
                W[w][h]["S" + s][1]().wait_recv()
                go(W[w][h]["F" + s])
                go(W[w][h][a, "T+"]), go(W[w][h][a, "T-"])

    def e24(w, a):
        for s in ("+", "-"):
            for h in (0, 1):
                W[w][h][a, "T" + s][1]().wait_recv()
                go(W[w][h][a, "G" + s])

    def e3(w):
        for s, q in (("+", 0), ("-", 1)):
            for h in (0, 1):
                W[w][h]["F" + s][1]().wait_recv()
                go(W[w][h][2, "T+", q]), go(W[w][h][2, "T-", q])

    def e5(w):
        for s, q in (("+", 0), ("-", 1)):
            for h in (0, 1):
                W[w][h][2, "T" + s, q][1]().wait_recv()
                go(W[w][h][2, "G" + s])

    def landed(w, names):
        for h in (0, 1):
            for name in names:
                W[w][h][name][1]().wait_recv()

    own_far = [(0, "G+"), (0, "G-")]
    side_far = [(-1, "G+"), (-1, "G-"), (1, "G+"), (1, "G-"), (2, "T+", 1), (2, "T-", 0)]
    far_far = [(2, "G+"), (2, "G-")]

    def rows_of(t, half):
        return tok_v.at[t] if half is None else tok_v.at[t, pl.ds(512 * half, 512)]

    block = lambda d, core: mod4(x + d) * 2 + core
    T = {}

    def token_copy(name, d_sent, half, peer, d_landed, core_landed):
        k = len(T)
        sent, got = rows_of(block(d_sent, c), half), rows_of(block(d_landed, core_landed), half)
        T[name] = remote(sent, sent, got, t_send.at[k], t_recv.at[k], peer)

    for half in (0, 1):
        token_copy(("X+", half), 0, half, to_x(1), -1, c)
        token_copy(("X-", half), 0, half, to_x(-1), 1, c)
    token_copy("Y+", -1, 0, to_x(1), 2, c)
    token_copy("Y-", 1, 1, to_x(-1), 2, c)
    token_copy(("D", 0), 0, None, partner, 0, 1 - c)
    token_copy(("D", -1), -1, None, partner, -1, 1 - c)
    token_copy(("D", 1), 1, None, partner, 1, 1 - c)
    token_copy(("D", 2, 0), 2, 0, partner, 2, 1 - c)
    token_copy(("D", 2, 1), 2, 1, partner, 2, 1 - c)

    loads[0].wait()
    loads[1].wait()
    gain = jnp.transpose(jnp.broadcast_to(gain_v[...], (128, 128)))
    for h in (0, 1):
        for k in range(4):
            cols = slice(512 * h + 128 * k, 512 * h + 128 * k + 128)
            up_v[h, pl.ds(pl.multiple_of(fs * 128, 128), 128), 128 * k : 128 * k + 128] = (gain * up32[:, cols]).astype(BF)
    loads[2].wait()
    pl.semaphore_wait(barrier, 7)

    e0(UP)
    go(T["X+", 0]), go(T["X-", 1]), go(T["X+", 1]), go(T["X-", 0])
    go(T["D", 0])

    loads[3].wait()
    for k in range(8):
        dn_v[fs, 128 * k : 128 * k + 128, :] = jnp.transpose(dn32[:, 128 * k : 128 * k + 128]).astype(BF)

    e1(UP)
    T["X+", 0][1]().wait_recv()
    go(T["Y+"])
    T["X-", 1][1]().wait_recv()
    go(T["Y-"])
    e24(UP, 0)
    e3(UP)
    T["X+", 1][1]().wait_recv()
    go(T["D", -1])
    T["X-", 0][1]().wait_recv()
    go(T["D", 1])
    e24(UP, -1)
    e24(UP, 1)
    e5(UP)
    e0(DN)
    T["Y+"][1]().wait_recv()
    go(T["D", 2, 0])
    T["Y-"][1]().wait_recv()
    go(T["D", 2, 1])
    for name in (("D", 0), ("D", -1), ("D", 1), ("D", 2, 0), ("D", 2, 1)):
        T[name][1]().wait_recv()

    def factor(m, carry):
        rows = pl.ds(pl.multiple_of(m * 128, 128), 128)
        total = jnp.zeros((128, 128), F32)
        for t in range(8):
            v = tok_v[t, rows, :].astype(F32)
            total += v[:, :128] * v[:, :128] + v[:, 128:] * v[:, 128:]
        mean = jnp.sum(total, axis=1, keepdims=True) * (1.0 / D)
        scale_v[rows, :] = jnp.broadcast_to(lax.rsqrt(mean + norm_floor), (128, 128))
        return carry

    lax.fori_loop(0, ROWS // 128, factor, 0)

    def hidden_half(h):
        def tile(m, carry):
            rows = pl.ds(pl.multiple_of(m * TILE, TILE), TILE)
            total = jnp.zeros((TILE, 512), F32)
            for t in range(8):
                total += jnp.dot(tok_v[t, rows, :], up_v[h, 256 * t : 256 * t + 256, :], preferred_element_type=F32)
            factor_of = scale_v[rows, :]
            for k in range(4):
                v = jnp.maximum(total[:, 128 * k : 128 * k + 128] * factor_of, 0.0)
                hid[rows, 512 * h + 128 * k : 512 * h + 128 * k + 128] = (v * v).astype(BF)
            return carry

        lax.fori_loop(0, ROWS // TILE, tile, 0)

    landed(UP, own_far + side_far + far_far)
    hidden_half(0)
    e1(DN)
    hidden_half(1)
    e24(DN, 0)

    near = y // 2

    def remote_partial(dz, o):
        slot = pbuf.at[o, dz]
        return remote(slot, prx.at[dz], prx.at[dz], r_send.at[dz], r_recv.at[dz], partner)

    def core_of(o):
        return near if o == 0 else 1 - near

    def product(dz, o):
        t = mod4(z + dz) * 2 + core_of(o)

        def tile(m, carry):
            rows = pl.ds(pl.multiple_of(m * TILE, TILE), TILE)
            pair = jnp.concatenate([dn_v[2 * t], dn_v[2 * t + 1]], axis=1)
            pbuf[o, dz, rows, :] = jnp.dot(hid[rows, :], pair, preferred_element_type=F32).astype(BF)
            return carry

        lax.fori_loop(0, ROWS // TILE, tile, 0)

        @pl.when(core_of(o) != c)
        def _():
            remote_partial(dz, o)[0]().start()

    half_rows = lambda ref, q: ref.at[pl.ds(512 * q, 512)]
    def ring(sign):
        q, k = (0, 4) if sign == 1 else (1, 7)
        side = 0 if sign == 1 else 1
        first = lambda src: remote(half_rows(src, q), fwd.at[side], fwd.at[side], r_send.at[k], r_recv.at[k], to_x(sign))
        second = remote(qf.at[side], half_rows(fin.at[side], q), half_rows(fin.at[side], q), r_send.at[k + 1], r_recv.at[k + 1], to_x(sign))
        direct = lambda src: remote(half_rows(src, 1 - q), half_rows(fin.at[side], 1 - q), half_rows(fin.at[side], 1 - q), r_send.at[k + 2], r_recv.at[k + 2], to_x(sign))
        return first, second, direct

    RING = {1: ring(1), -1: ring(-1)}
    ahead = lambda dz: mod4(z + dz - x)

    def reduce_pair(dz, o):
        @pl.when(core_of(o) == c)
        def _():
            remote_partial(dz, o)[1]().wait_recv()

            def tile(m, carry):
                rows = pl.ds(pl.multiple_of(m * TILE, TILE), TILE)
                pbuf[o, dz, rows, :] = (pbuf[o, dz, rows, :].astype(F32) + prx[dz, rows, :].astype(F32)).astype(BF)
                return carry

            lax.fori_loop(0, ROWS // TILE, tile, 0)

            @pl.when(ahead(dz) == 2)
            def _():
                RING[1][0](pbuf.at[o, dz])[0]().start()
                RING[-1][0](pbuf.at[o, dz])[0]().start()

            for sign, d in ((1, 1), (-1, 3)):
                @pl.when(ahead(dz) == d)
                def _():
                    RING[sign][2](pbuf.at[o, dz])[0]().start()

    def forward(dz, o):
        @pl.when(core_of(o) == c)
        def _():
            for sign, d in ((1, 1), (-1, 3)):
                side, q = (0, 0) if sign == 1 else (1, 1)

                @pl.when(ahead(dz) == d)
                def _():
                    RING[sign][0](pbuf.at[o, dz])[1]().wait_recv()

                    def tile(m, carry):
                        at = m * TILE
                        here = pl.ds(pl.multiple_of(at, TILE), TILE)
                        mine = pl.ds(pl.multiple_of(512 * q + at, TILE), TILE)
                        qf[side, here, :] = (pbuf[o, dz, mine, :].astype(F32) + fwd[side, here, :].astype(F32)).astype(BF)
                        return carry

                    lax.fori_loop(0, 512 // TILE, tile, 0)
                    RING[sign][1][0]().start()

    product(0, 0)
    e3(DN)
    reduce_pair(0, 0)
    e24(DN, -1)
    e24(DN, 1)
    product(1, 0)
    product(3, 0)
    reduce_pair(1, 0)
    forward(0, 0)
    reduce_pair(3, 0)
    e5(DN)
    landed(DN, own_far)
    product(0, 1)
    forward(1, 0)
    reduce_pair(0, 1)
    forward(3, 0)
    landed(DN, side_far)
    product(2, 0)
    product(1, 1)
    reduce_pair(2, 0)
    product(3, 1)
    forward(0, 1)
    reduce_pair(1, 1)
    landed(DN, far_far)
    product(2, 1)
    reduce_pair(3, 1)
    forward(2, 0)
    forward(1, 1)
    reduce_pair(2, 1)
    forward(3, 1)
    forward(2, 1)

    mine = mod4(x - z)
    o_mine = jnp.where(near == c, 0, 1)
    for sign in (1, -1):
        RING[sign][1][1]().wait_recv()
        RING[sign][2](pbuf.at[0, 0])[1]().wait_recv()

    def last(m, carry):
        rows = pl.ds(pl.multiple_of(m * TILE, TILE), TILE)
        total = pbuf[o_mine, mine, rows, :].astype(F32) + fin[0, rows, :].astype(F32) + fin[1, rows, :].astype(F32)
        out_v[rows, :] = total.astype(BF)
        return carry

    lax.fori_loop(0, ROWS // TILE, last, 0)

    for send in sends:
        send.wait_send()
    for dz in range(4):
        remote_partial(dz, 0)[0]().wait_send()
    for sign in (1, -1):
        RING[sign][0](pbuf.at[0, 0])[0]().wait_send()
        RING[sign][1][0]().wait_send()
        RING[sign][2](pbuf.at[0, 0])[0]().wait_send()


def put_out(up_v, dn_v, out_v, up_out, dn_out, out, sem):
    copies = [pltpu.make_async_copy(out_v, out, sem.at[18])]
    for h in (0, 1):
        copies.append(pltpu.make_async_copy(up_v.at[h], up_out.at[:, pl.ds(512 * h, 512)], sem.at[h]))
    for f in range(16):
        copies.append(pltpu.make_async_copy(dn_v.at[f], dn_out.at[:, pl.ds(128 * f, 128)], sem.at[2 + f]))
    for copy in copies:
        copy.start()
    for copy in copies:
        copy.wait()


def on_device(tokens, norm_gain, up_master, down_master):
    anywhere, vmem = pl.BlockSpec(memory_space=pl.ANY), pl.BlockSpec(memory_space=pltpu.VMEM)
    in_hbm = lambda v: pltpu.with_memory_space_constraint(v, pltpu.HBM)
    held = pl.pallas_call(
        kernel,
        name="gather_mlp",
        out_shape=(
            pltpu.VMEM((2, D, 512), BF),
            pltpu.VMEM((16, 1024, 128), BF),
            pltpu.VMEM((ROWS, 256), BF),
        ),
        in_specs=[anywhere] * 4,
        out_specs=(vmem, vmem, vmem),
        scratch_shapes=[
            pltpu.VMEM((128, 1024), F32),
            pltpu.VMEM((128, 1024), F32),
            pltpu.VMEM((1, 128), F32),
            pltpu.VMEM((8, ROWS, 256), BF),
            pltpu.VMEM((ROWS, 128), F32),
            pltpu.VMEM((ROWS, 1024), BF),
            pltpu.VMEM((2, 4, ROWS, 256), BF),
            pltpu.VMEM((4, ROWS, 256), BF),
            pltpu.VMEM((2, 512, 256), BF),
            pltpu.VMEM((2, 512, 256), BF),
            pltpu.VMEM((2, ROWS, 256), BF),
            pltpu.SemaphoreType.DMA((4,)),
            pltpu.SemaphoreType.DMA((2, 2, 22)),
            pltpu.SemaphoreType.DMA((2, 2, 22)),
            pltpu.SemaphoreType.DMA((11,)),
            pltpu.SemaphoreType.DMA((11,)),
            pltpu.SemaphoreType.DMA((10,)),
            pltpu.SemaphoreType.DMA((10,)),
        ],
        compiler_params=pltpu.CompilerParams(collective_id=0, has_side_effects=True, vmem_limit_bytes=40 << 20),
    )(in_hbm(tokens), in_hbm(norm_gain.reshape(1, 128)), in_hbm(up_master), in_hbm(down_master))
    return pl.pallas_call(
        put_out,
        name="put_out",
        out_shape=(
            jax.ShapeDtypeStruct((D, 1024), BF),
            jax.ShapeDtypeStruct((1024, D), BF),
            jax.ShapeDtypeStruct((ROWS, 256), BF),
        ),
        in_specs=[vmem] * 3,
        out_specs=(anywhere,) * 3,
        scratch_shapes=[pltpu.SemaphoreType.DMA((19,))],
        compiler_params=pltpu.CompilerParams(vmem_limit_bytes=16 << 20),
    )(*held)


def solution(mesh):
    in_specs = (P("fs", "tp"), P("fs"), P("fs", "tp"), P("fs", "tp"))
    out_specs = (P(None, "tp"), P("tp", None), P("fs", "tp"))
    return jax.shard_map(
        on_device, mesh=mesh, in_specs=in_specs, out_specs=out_specs, check_vma=False
    )
```

time: 187 us -> 87.1 us (0.47)
  the two profiles are of different devices: /device:TPU:0 before, /device:TPU:5 now
where the time goes in v1:
time: 87.1 us; the launch traced here: 85.5 us
  Pallas kernels  84.9 us (97%)
    pallas_call x1, Pallas kernels, on_device(): pl.pallas_call(kernel, name='gather_mlp', out_shape=(pltpu.VMEM((2, D, 51...  81.3 us
    pallas_call x1, Pallas kernels, on_device(): pl.pallas_call(put_out, name='put_out', out_shape=(jax.ShapeDtypeStruct((...  3.6 us

profile of v1, /device:TPU:5, one launch (start us, length us, event | category | flops | bytes accessed | tf_op | source)
XLA Modules:
  0.0 85.5 jit_solution(8233087331689052070)
XLA Ops:
  0.6 81.3 %gather_mlp.1 = (bf16[2,2048,512]{2,1,0:T(8,128)(2,1)S(1)}, bf16[16,1024,128]{2,1,0:T(8,128)(2,1)S(1)}, bf16[1024,256]{1,0:T(8,128)(2,1)S(1)}) custom-call(bf16[1024,256]{1,0:T(8,128)(2,1)} %tok_in.1, f32[1,128]{1,0:T(1,128)} %bitcast.1, f32[128,1024]{1,0:T(8,128)} %up_in.1, f32[128,1024]{1,0:T(8,128)} %dn_in.1), custom_call_target="tpu_custom_call" | custom-call | tf_op jit(solution)/shard_map/gather_mlp/pallas_call | solution.py:373
  81.9 3.6 %put_out.1 = (bf16[2048,1024]{1,0:T(8,128)(2,1)}, bf16[1024,2048]{1,0:T(8,128)(2,1)}, bf16[1024,256]{1,0:T(8,128)(2,1)}) custom-call(bf16[2,2048,512]{2,1,0:T(8,128)(2,1)S(1)} %get-tuple-element.6.up_v, bf16[16,1024,128]{2,1,0:T(8,128)(2,1)S(1)} %get-tuple-element.7.dn_v, bf16[1024,256]{1,0:T(8,128)(2,1)S(1)} %get-tuple-element.8.out_v), custom_call_target="tpu_custom_call" | custom-call | tf_op jit(solution)/shard_map/put_out/pallas_call | solution.py:405

commit v2 on v1

v2 whole, which is shorter than its diff:
```python
import jax
import jax.numpy as jnp
from jax import lax
from jax.experimental import pallas as pl
from jax.experimental.pallas import tpu as pltpu
from jax.sharding import PartitionSpec as P

norm_floor = 1e-06

MESH = pl.DeviceIdType.MESH
BF, F32 = jnp.bfloat16, jnp.float32
D, FF = 2048, 8192
ROWS = 1024
TILE = 512
UP, DN = 0, 1


def kernel(
    tok_in, gain_in, up_in, dn_in,
    up_v, dn_v, out_v,
    up32, dn32, gain_v, tok_v, scale_v, acc, hid, pbuf, prx, fwd, qf, fin,
    in_sem, w_send, w_recv, t_send, t_recv, p_send, p_recv, r_send, r_recv,
):
    fs, tp = lax.axis_index("fs"), lax.axis_index("tp")
    z, y, x, c = fs // 4, fs % 4, tp // 2, tp % 2
    mod4 = lambda v: lax.rem(v + 8, 4)
    to_y = lambda s: {"fs": z * 4 + mod4(y + s), "tp": tp}
    to_z = lambda s: {"fs": mod4(z + s) * 4 + y, "tp": tp}
    to_x = lambda s: {"fs": fs, "tp": mod4(x + s) * 2 + c}
    partner = {"fs": fs, "tp": x * 2 + 1 - c}

    loads = [
        pltpu.make_async_copy(up_in, up32, in_sem.at[0]),
        pltpu.make_async_copy(gain_in, gain_v, in_sem.at[1]),
        pltpu.make_async_copy(tok_in, tok_v.at[tp], in_sem.at[2]),
        pltpu.make_async_copy(dn_in, dn32, in_sem.at[3]),
    ]
    for load in loads:
        load.start()
    barrier = pltpu.get_barrier_semaphore()
    for peer in (to_y(1), to_y(-1), to_z(1), to_z(-1), to_x(1), to_x(-1), partner):
        pl.semaphore_signal(barrier, inc=1, device_id=peer, device_id_type=MESH)

    sends = []

    def remote(src, dst, landed, send_sem, recv_sem, peer):
        out = lambda: pltpu.make_async_remote_copy(src, dst, send_sem, recv_sem, peer, MESH)
        back = lambda: pltpu.make_async_remote_copy(landed, landed, send_sem, recv_sem, peer, MESH)
        return out, back

    def go(pair):
        copy = pair[0]()
        copy.start()
        sends.append(copy)

    toward = 1 - 2 * (y % 2)
    y_at = {0: 0, "+": toward, "-": -toward, 2: 2}

    def weight_copies(w):
        def piece(h, jy, jz, q):
            f = mod4(z + jz) * 4 + mod4(y + y_at[jy])
            if w == UP:
                at, n = f * 128 + (0 if q is None else 64 * q), 128 if q is None else 64
                return up_v.at[h, pl.ds(pl.multiple_of(at, 64), n)]
            at, n = 512 * h + (0 if q is None else 256 * q), 512 if q is None else 256
            return dn_v.at[f, pl.ds(at, n)]

        tables = ({}, {})

        def add(h, name, sent, side, landed):
            k = len(tables[h])
            peer = to_y(y_at[side]) if side in ("+", "-") else to_z(side)
            src, got = piece(h, *sent), piece(h, *landed)
            tables[h][name] = remote(src, src, got, w_send.at[w, h, k], w_recv.at[w, h, k], peer)

        for s, other, q in (("+", "-", 1), ("-", "+", 0)):
            add(0, ("S", s), (0, 0, None), s, (s, 0, None))
            add(0, ("F", s), (other, 0, q), s, (2, 0, q))
            for jz in (0, 1, -1):
                add(1, (jz, "T", s), (0, jz, None), s, (s, jz, None))
                add(1, (jz, "G", s), (other, jz, q), s, (2, jz, q))
            for part in (0, 1):
                add(1, (2, "T", s, part), (0, 2, part), s, (s, 2, part))
            add(1, (2, "G", s), (other, 2, q), s, (2, 2, q))
        for s, q in ((1, 0), (-1, 1)):
            add(1, ("S", s), (0, 0, None), s, (0, -s, None))
            add(1, ("F", s), (0, -s, q), s, (0, 2, q))
            for jy in (0, "+", "-"):
                add(0, (jy, "T", s), (jy, 0, None), s, (jy, -s, None))
                add(0, (jy, "G", s), (jy, -s, q), s, (jy, 2, q))
            for part in (0, 1):
                add(0, (2, "T", s, part), (2, 0, part), s, (2, -s, part))
            add(0, (2, "G", s), (2, -s, q), s, (2, 2, q))
        return tables

    W = [weight_copies(w) for w in (UP, DN)]

    def take(w, h, *names):
        for name in names:
            W[w][h][name][1]().wait_recv()

    def put(w, h, *names):
        for name in names:
            go(W[w][h][name])

    def e0y(w):
        put(w, 0, ("S", "+"), ("S", "-"))
        put(w, 1, (0, "T", "+"), (0, "T", "-"))

    def e0z(w):
        put(w, 1, ("S", 1), ("S", -1))
        put(w, 0, (0, "T", 1), (0, "T", -1))

    def e1(w):
        take(w, 0, ("S", "+"))
        put(w, 0, ("+", "T", 1), ("+", "T", -1), ("F", "-"))
        for s in (1, -1):
            take(w, 1, ("S", s))
            put(w, 1, (-s, "T", "+"), (-s, "T", "-"), ("F", s))
        take(w, 0, ("S", "-"))
        put(w, 0, ("F", "+"))

    def e2(w):
        for s in (1, -1):
            take(w, 0, (0, "T", s))
            put(w, 0, (0, "G", s))
        take(w, 1, (0, "T", "+"))
        put(w, 1, (0, "G", "-"))
        take(w, 1, (0, "T", "-"))

    def e3a(w):
        for s in (1, -1):
            take(w, 0, ("+", "T", s))
            put(w, 0, ("+", "G", s))

    def e3b(w):
        for s, q in ((1, 0), (-1, 1)):
            take(w, 1, ("F", s))
            put(w, 1, (2, "T", "+", q), (2, "T", "-", q))
        put(w, 0, ("-", "T", 1), ("-", "T", -1))
        put(w, 1, (0, "G", "+"))

    def e3c(w):
        for s, q in (("-", 0), ("+", 1)):
            take(w, 0, ("F", s))
            put(w, 0, (2, "T", 1, q), (2, "T", -1, q))

    def e4a(w):
        for jz in (-1, 1):
            for s, other in (("+", "-"), ("-", "+")):
                take(w, 1, (jz, "T", s))
                put(w, 1, (jz, "G", other))

    def own_far(w):
        take(w, 0, (0, "G", 1), (0, "G", -1), ("+", "G", 1), ("+", "G", -1))
        take(w, 1, (2, "T", "+", 0))
        put(w, 1, (2, "G", "-"))
        take(w, 1, (2, "T", "+", 1))

    def e4b(w):
        take(w, 1, (2, "T", "-", 1))
        put(w, 1, (2, "G", "+"))

    def e4c(w):
        for s in (1, -1):
            take(w, 0, ("-", "T", s))
            put(w, 0, ("-", "G", s))

    def e4d(w):
        for s, q in ((1, 0), (-1, 1)):
            take(w, 0, (2, "T", s, q))
            put(w, 0, (2, "G", s))

    def other_near(w):
        take(w, 1, (0, "G", "+"), (0, "G", "-"))

    def other_side(w):
        take(w, 0, (2, "T", 1, 1), (2, "T", -1, 0))
        take(w, 1, *[(jz, "G", s) for jz in (1, -1) for s in ("+", "-")])

    def other_far(w):
        take(w, 0, ("-", "G", 1), ("-", "G", -1), (2, "G", 1), (2, "G", -1))
        take(w, 1, (2, "T", "-", 0), (2, "G", "+"), (2, "G", "-"))

    def rows_of(t, half):
        return tok_v.at[t] if half is None else tok_v.at[t, pl.ds(512 * half, 512)]

    block = lambda d, core: mod4(x + d) * 2 + core
    T = {}

    def token_copy(name, d_sent, half, peer, d_landed, core_landed):
        k = len(T)
        sent, got = rows_of(block(d_sent, c), half), rows_of(block(d_landed, core_landed), half)
        T[name] = remote(sent, sent, got, t_send.at[k], t_recv.at[k], peer)

    for half in (0, 1):
        token_copy(("X+", half), 0, half, to_x(1), -1, c)
        token_copy(("X-", half), 0, half, to_x(-1), 1, c)
    token_copy("Y+", -1, 0, to_x(1), 2, c)
    token_copy("Y-", 1, 1, to_x(-1), 2, c)
    token_copy(("D", 0), 0, None, partner, 0, 1 - c)
    token_copy(("D", -1), -1, None, partner, -1, 1 - c)
    token_copy(("D", 1), 1, None, partner, 1, 1 - c)
    token_copy(("D", 2, 0), 2, 0, partner, 2, 1 - c)
    token_copy(("D", 2, 1), 2, 1, partner, 2, 1 - c)

    loads[0].wait()
    loads[1].wait()
    gain = jnp.transpose(jnp.broadcast_to(gain_v[...], (128, 128)))
    for h in (0, 1):
        for k in range(4):
            cols = slice(512 * h + 128 * k, 512 * h + 128 * k + 128)
            up_v[h, pl.ds(pl.multiple_of(fs * 128, 128), 128), 128 * k : 128 * k + 128] = (gain * up32[:, cols]).astype(BF)
    loads[2].wait()
    pl.semaphore_wait(barrier, 7)

    e0y(UP)
    e0z(UP)
    go(T["X+", 0]), go(T["X-", 1]), go(T["X+", 1]), go(T["X-", 0])
    go(T["D", 0])

    loads[3].wait()
    for k in range(8):
        dn_v[fs, 128 * k : 128 * k + 128, :] = jnp.transpose(dn32[:, 128 * k : 128 * k + 128]).astype(BF)

    e1(UP)
    e2(UP)
    T["X+", 0][1]().wait_recv()
    go(T["Y+"])
    T["X-", 1][1]().wait_recv()
    go(T["Y-"])
    e3a(UP)
    e3b(UP)
    e4a(UP)
    T["X+", 1][1]().wait_recv()
    go(T["D", -1])
    T["X-", 0][1]().wait_recv()
    go(T["D", 1])
    e3c(UP)
    e4c(UP)
    own_far(UP)
    e4b(UP)
    e0y(DN)
    T["Y+"][1]().wait_recv()
    go(T["D", 2, 0])
    T["Y-"][1]().wait_recv()
    go(T["D", 2, 1])
    e4d(UP)
    e0z(DN)
    for name in (("D", 0), ("D", -1), ("D", 1), ("D", 2, 0), ("D", 2, 1)):
        T[name][1]().wait_recv()

    def factor(m, carry):
        rows = pl.ds(pl.multiple_of(m * 128, 128), 128)
        total = jnp.zeros((128, 128), F32)
        for t in range(8):
            v = tok_v[t, rows, :].astype(F32)
            total += v[:, :128] * v[:, :128] + v[:, 128:] * v[:, 128:]
        mean = jnp.sum(total, axis=1, keepdims=True) * (1.0 / D)
        scale_v[rows, :] = jnp.broadcast_to(lax.rsqrt(mean + norm_floor), (128, 128))
        return carry

    lax.fori_loop(0, ROWS // 128, factor, 0)

    near = y // 2

    def core_of(o):
        return near if o == 0 else 1 - near

    def pair_of(dz, o):
        return mod4(z + dz) * 2 + core_of(o)

    def dots(h, rows, pairs):
        total = None
        for pair in pairs:
            t = pair_of(*pair)
            weights = up_v[h, pl.ds(pl.multiple_of(256 * t, 256), 256), :]
            term = jnp.dot(tok_v[t, rows, :], weights, preferred_element_type=F32)
            total = term if total is None else total + term
        return total

    def first_part(i, carry):
        h, m = i // (ROWS // TILE), lax.rem(i, ROWS // TILE)
        rows = pl.ds(pl.multiple_of(m * TILE, TILE), TILE)
        acc[h, rows, :] = dots(h, rows, ((0, 0), (1, 0), (3, 0), (2, 0)))
        return carry

    def second_part(h):
        def tile(m, carry):
            rows = pl.ds(pl.multiple_of(m * TILE, TILE), TILE)
            total = acc[h, rows, :] + dots(h, rows, ((0, 1), (1, 1), (3, 1), (2, 1)))
            factor_of = scale_v[rows, :]
            for k in range(4):
                v = jnp.maximum(total[:, 128 * k : 128 * k + 128] * factor_of, 0.0)
                hid[rows, 512 * h + 128 * k : 512 * h + 128 * k + 128] = (v * v).astype(BF)
            return carry

        lax.fori_loop(0, ROWS // TILE, tile, 0)

    lax.fori_loop(0, 2 * ROWS // TILE, first_part, 0)
    other_near(UP)
    other_side(UP)
    other_far(UP)
    second_part(0)
    e1(DN)
    second_part(1)
    e2(DN)

    def remote_partial(dz, o, r):
        part = pl.ds(pl.multiple_of(512 * r, 512), 512)
        return remote(pbuf.at[o, dz, part], prx.at[dz, part], prx.at[dz, part], p_send.at[dz, r], p_recv.at[dz, r], partner)

    def product(dz, o):
        t = pair_of(dz, o)

        def tile(r, carry):
            rows = pl.ds(pl.multiple_of(r * 512, 512), 512)
            pair = jnp.concatenate([dn_v[2 * t], dn_v[2 * t + 1]], axis=1)
            pbuf[o, dz, rows, :] = jnp.dot(hid[rows, :], pair, preferred_element_type=F32).astype(BF)

            @pl.when(core_of(o) != c)
            def _():
                remote_partial(dz, o, r)[0]().start()

            return carry

        lax.fori_loop(0, 2, tile, 0)

    def ring(sign):
        side = 0 if sign == 1 else 1
        q, k, peer = side, 5 * side, to_x(sign)
        chunk = lambda ref, base, j: ref.at[pl.ds(base + 256 * j, 256)]

        def first(src, j):
            got = chunk(fwd.at[side], 0, j)
            return remote(chunk(src, 512 * q, j), got, got, r_send.at[k + j], r_recv.at[k + j], peer)

        def second(j):
            got = chunk(fin.at[side], 512 * q, j)
            return remote(chunk(qf.at[side], 0, j), got, got, r_send.at[k + 2 + j], r_recv.at[k + 2 + j], peer)

        def direct(src):
            rows = pl.ds(512 * (1 - q), 512)
            return remote(src.at[rows], fin.at[side, rows], fin.at[side, rows], r_send.at[k + 4], r_recv.at[k + 4], peer)

        return first, second, direct

    RING = {1: ring(1), -1: ring(-1)}
    ahead = lambda dz: mod4(z + dz - x)

    def reduce_pair(dz, o):
        @pl.when(core_of(o) == c)
        def _():
            mine = pbuf.at[o, dz]
            for r, sign, d in ((0, 1, 3), (1, -1, 1)):
                remote_partial(dz, o, r)[1]().wait_recv()
                rows = pl.ds(512 * r, 512)
                pbuf[o, dz, rows, :] = (pbuf[o, dz, rows, :].astype(F32) + prx[dz, rows, :].astype(F32)).astype(BF)

                @pl.when(ahead(dz) == 2)
                def _():
                    RING[sign][0](mine, 0)[0]().start()
                    RING[sign][0](mine, 1)[0]().start()

                @pl.when(ahead(dz) == d)
                def _():
                    RING[-sign][2](mine)[0]().start()

    def forward(dz, o):
        @pl.when(core_of(o) == c)
        def _():
            for sign, d in ((1, 1), (-1, 3)):
                side = 0 if sign == 1 else 1

                @pl.when(ahead(dz) == d)
                def _():
                    for j in (0, 1):
                        RING[sign][0](pbuf.at[o, dz], j)[1]().wait_recv()
                        here, mine = pl.ds(256 * j, 256), pl.ds(512 * side + 256 * j, 256)
                        qf[side, here, :] = (pbuf[o, dz, mine, :].astype(F32) + fwd[side, here, :].astype(F32)).astype(BF)
                        RING[sign][1](j)[0]().start()

    product(0, 0)
    e3a(DN)
    reduce_pair(0, 0)
    e3b(DN)
    e4a(DN)
    product(1, 0)
    forward(0, 0)
    product(3, 0)
    e3c(DN)
    reduce_pair(1, 0)
    reduce_pair(3, 0)
    e4c(DN)
    own_far(DN)
    product(2, 0)
    e4b(DN)
    other_near(DN)
    product(0, 1)
    reduce_pair(2, 0)
    e4d(DN)
    other_side(DN)
    product(1, 1)
    reduce_pair(0, 1)
    product(3, 1)
    reduce_pair(1, 1)
    other_far(DN)
    product(2, 1)
    forward(3, 0)
    forward(1, 0)
    reduce_pair(3, 1)
    forward(2, 0)
    reduce_pair(2, 1)
    forward(0, 1)
    forward(1, 1)
    forward(3, 1)
    forward(2, 1)

    mine = mod4(x - z)
    o_mine = jnp.where(near == c, 0, 1)
    for sign in (1, -1):
        RING[sign][1](0)[1]().wait_recv()
        RING[sign][1](1)[1]().wait_recv()
        RING[sign][2](pbuf.at[0, 0])[1]().wait_recv()

    def last(m, carry):
        rows = pl.ds(pl.multiple_of(m * TILE, TILE), TILE)
        total = pbuf[o_mine, mine, rows, :].astype(F32) + fin[0, rows, :].astype(F32) + fin[1, rows, :].astype(F32)
        out_v[rows, :] = total.astype(BF)
        return carry

    lax.fori_loop(0, ROWS // TILE, last, 0)

    for send in sends:
        send.wait_send()
    for dz in range(4):
        for r in (0, 1):
            remote_partial(dz, 0, r)[0]().wait_send()
    for sign in (1, -1):
        for j in (0, 1):
            RING[sign][0](pbuf.at[0, 0], j)[0]().wait_send()
            RING[sign][1](j)[0]().wait_send()
        RING[sign][2](pbuf.at[0, 0])[0]().wait_send()


def put_out(up_v, dn_v, out_v, up_out, dn_out, out, sem):
    copies = [pltpu.make_async_copy(out_v, out, sem.at[18])]
    for h in (0, 1):
        copies.append(pltpu.make_async_copy(up_v.at[h], up_out.at[:, pl.ds(512 * h, 512)], sem.at[h]))
    for f in range(16):
        copies.append(pltpu.make_async_copy(dn_v.at[f], dn_out.at[:, pl.ds(128 * f, 128)], sem.at[2 + f]))
    for copy in copies:
        copy.start()
    for copy in copies:
        copy.wait()


def on_device(tokens, norm_gain, up_master, down_master):
    anywhere, vmem = pl.BlockSpec(memory_space=pl.ANY), pl.BlockSpec(memory_space=pltpu.VMEM)
    in_hbm = lambda v: pltpu.with_memory_space_constraint(v, pltpu.HBM)
    held = pl.pallas_call(
        kernel,
        name="gather_mlp",
        out_shape=(
            pltpu.VMEM((2, D, 512), BF),
            pltpu.VMEM((16, 1024, 128), BF),
            pltpu.VMEM((ROWS, 256), BF),
        ),
        in_specs=[anywhere] * 4,
        out_specs=(vmem, vmem, vmem),
        scratch_shapes=[
            pltpu.VMEM((128, 1024), F32),
            pltpu.VMEM((128, 1024), F32),
            pltpu.VMEM((1, 128), F32),
            pltpu.VMEM((8, ROWS, 256), BF),
            pltpu.VMEM((ROWS, 128), F32),
            pltpu.VMEM((2, ROWS, 512), F32),
            pltpu.VMEM((ROWS, 1024), BF),
            pltpu.VMEM((2, 4, ROWS, 256), BF),
            pltpu.VMEM((4, ROWS, 256), BF),
            pltpu.VMEM((2, 512, 256), BF),
            pltpu.VMEM((2, 512, 256), BF),
            pltpu.VMEM((2, ROWS, 256), BF),
            pltpu.SemaphoreType.DMA((4,)),
            pltpu.SemaphoreType.DMA((2, 2, 22)),
            pltpu.SemaphoreType.DMA((2, 2, 22)),
            pltpu.SemaphoreType.DMA((11,)),
            pltpu.SemaphoreType.DMA((11,)),
            pltpu.SemaphoreType.DMA((4, 2)),
            pltpu.SemaphoreType.DMA((4, 2)),
            pltpu.SemaphoreType.DMA((10,)),
            pltpu.SemaphoreType.DMA((10,)),
        ],
        compiler_params=pltpu.CompilerParams(collective_id=0, has_side_effects=True, vmem_limit_bytes=40 << 20),
    )(in_hbm(tokens), in_hbm(norm_gain.reshape(1, 128)), in_hbm(up_master), in_hbm(down_master))
    return pl.pallas_call(
        put_out,
        name="put_out",
        out_shape=(
            jax.ShapeDtypeStruct((D, 1024), BF),
            jax.ShapeDtypeStruct((1024, D), BF),
            jax.ShapeDtypeStruct((ROWS, 256), BF),
        ),
        in_specs=[vmem] * 3,
        out_specs=(anywhere,) * 3,
        scratch_shapes=[pltpu.SemaphoreType.DMA((19,))],
        compiler_params=pltpu.CompilerParams(vmem_limit_bytes=16 << 20),
    )(*held)


def solution(mesh):
    in_specs = (P("fs", "tp"), P("fs"), P("fs", "tp"), P("fs", "tp"))
    out_specs = (P(None, "tp"), P("tp", None), P("fs", "tp"))
    return jax.shard_map(
        on_device, mesh=mesh, in_specs=in_specs, out_specs=out_specs, check_vma=False
    )
```

time: 87.1 us -> 74.1 us (0.85); the launches traced: 85.5 us -> 74 us
  Pallas kernels: 84.9 us -> 73.4 us
    pallas_call x1, Pallas kernels: 81.3 us -> 69.8 us  [on_device(): pl.pallas_call(kernel, name='gather_mlp', out_shape=(pltpu.VMEM((2, D, 51...]
where the time goes in v2:
time: 74.1 us; the launch traced here: 74 us
  Pallas kernels  73.4 us (99%)
    pallas_call x1, Pallas kernels, on_device(): pl.pallas_call(kernel, name='gather_mlp', out_shape=(pltpu.VMEM((2, D, 51...  69.8 us
    pallas_call x1, Pallas kernels, on_device(): pl.pallas_call(put_out, name='put_out', out_shape=(jax.ShapeDtypeStruct((...  3.6 us

profile of v2, /device:TPU:5, one launch (start us, length us, event | category | flops | bytes accessed | tf_op | source)
XLA Modules:
  0.0 74.0 jit_solution(4282207251744351856)
XLA Ops:
  0.6 69.8 %gather_mlp.1 = (bf16[2,2048,512]{2,1,0:T(8,128)(2,1)S(1)}, bf16[16,1024,128]{2,1,0:T(8,128)(2,1)S(1)}, bf16[1024,256]{1,0:T(8,128)(2,1)S(1)}) custom-call(bf16[1024,256]{1,0:T(8,128)(2,1)} %tok_in.1, f32[1,128]{1,0:T(1,128)} %bitcast.1, f32[128,1024]{1,0:T(8,128)} %up_in.1, f32[128,1024]{1,0:T(8,128)} %dn_in.1), custom_call_target="tpu_custom_call" | custom-call | tf_op jit(solution)/shard_map/gather_mlp/pallas_call | solution.py:461
  70.4 3.6 %put_out.1 = (bf16[2048,1024]{1,0:T(8,128)(2,1)}, bf16[1024,2048]{1,0:T(8,128)(2,1)}, bf16[1024,256]{1,0:T(8,128)(2,1)}) custom-call(bf16[2,2048,512]{2,1,0:T(8,128)(2,1)S(1)} %get-tuple-element.6.up_v, bf16[16,1024,128]{2,1,0:T(8,128)(2,1)S(1)} %get-tuple-element.7.dn_v, bf16[1024,256]{1,0:T(8,128)(2,1)S(1)} %get-tuple-element.8.out_v), custom_call_target="tpu_custom_call" | custom-call | tf_op jit(solution)/shard_map/put_out/pallas_call | solution.py:496

commit v3 on v2

--- a/solution.py
+++ b/solution.py
@@ -19,7 +19,7 @@
     tok_in, gain_in, up_in, dn_in,
     up_v, dn_v, out_v,
     up32, dn32, gain_v, tok_v, scale_v, acc, hid, pbuf, prx, fwd, qf, fin,
-    in_sem, w_send, w_recv, t_send, t_recv, p_send, p_recv, r_send, r_recv,
+    in_sem, sent_sem, w_recv, t_recv, p_recv, r_recv,
 ):
     fs, tp = lax.axis_index("fs"), lax.axis_index("tp")
     z, y, x, c = fs // 4, fs % 4, tp // 2, tp % 2
@@ -41,17 +41,13 @@
     for peer in (to_y(1), to_y(-1), to_z(1), to_z(-1), to_x(1), to_x(-1), partner):
         pl.semaphore_signal(barrier, inc=1, device_id=peer, device_id_type=MESH)
 
-    sends = []
-
     def remote(src, dst, landed, send_sem, recv_sem, peer):
         out = lambda: pltpu.make_async_remote_copy(src, dst, send_sem, recv_sem, peer, MESH)
         back = lambda: pltpu.make_async_remote_copy(landed, landed, send_sem, recv_sem, peer, MESH)
         return out, back
 
     def go(pair):
-        copy = pair[0]()
-        copy.start()
-        sends.append(copy)
+        pair[0]().start()
 
     toward = 1 - 2 * (y % 2)
     y_at = {0: 0, "+": toward, "-": -toward, 2: 2}
@@ -71,7 +67,7 @@
             k = len(tables[h])
             peer = to_y(y_at[side]) if side in ("+", "-") else to_z(side)
             src, got = piece(h, *sent), piece(h, *landed)
-            tables[h][name] = remote(src, src, got, w_send.at[w, h, k], w_recv.at[w, h, k], peer)
+            tables[h][name] = remote(src, src, got, sent_sem.at[w], w_recv.at[w, h, k], peer)
 
         for s, other, q in (("+", "-", 1), ("-", "+", 0)):
             add(0, ("S", s), (0, 0, None), s, (s, 0, None))
@@ -191,7 +187,7 @@
     def token_copy(name, d_sent, half, peer, d_landed, core_landed):
         k = len(T)
         sent, got = rows_of(block(d_sent, c), half), rows_of(block(d_landed, core_landed), half)
-        T[name] = remote(sent, sent, got, t_send.at[k], t_recv.at[k], peer)
+        T[name] = remote(sent, sent, got, sent_sem.at[2], t_recv.at[k], peer)
 
     for half in (0, 1):
         token_copy(("X+", half), 0, half, to_x(1), -1, c)
@@ -231,36 +227,40 @@
     go(T["Y-"])
     e3a(UP)
     e3b(UP)
-    e4a(UP)
     T["X+", 1][1]().wait_recv()
     go(T["D", -1])
     T["X-", 0][1]().wait_recv()
     go(T["D", 1])
+    e4a(UP)
     e3c(UP)
     e4c(UP)
     own_far(UP)
-    e4b(UP)
-    e0y(DN)
     T["Y+"][1]().wait_recv()
     go(T["D", 2, 0])
     T["Y-"][1]().wait_recv()
     go(T["D", 2, 1])
+    e4b(UP)
+    e0y(DN)
     e4d(UP)
     e0z(DN)
     for name in (("D", 0), ("D", -1), ("D", 1), ("D", 2, 0), ("D", 2, 1)):
         T[name][1]().wait_recv()
 
+    ones = jnp.ones((128, 128), BF)
+
     def factor(m, carry):
-        rows = pl.ds(pl.multiple_of(m * 128, 128), 128)
-        total = jnp.zeros((128, 128), F32)
+        rows = pl.ds(pl.multiple_of(m * 256, 256), 256)
+        total = jnp.zeros((256, 128), F32)
         for t in range(8):
             v = tok_v[t, rows, :].astype(F32)
             total += v[:, :128] * v[:, :128] + v[:, 128:] * v[:, 128:]
-        mean = jnp.sum(total, axis=1, keepdims=True) * (1.0 / D)
-        scale_v[rows, :] = jnp.broadcast_to(lax.rsqrt(mean + norm_floor), (128, 128))
+        high = total.astype(BF)
+        low = (total - high.astype(F32)).astype(BF)
+        summed = jnp.dot(high, ones, preferred_element_type=F32) + jnp.dot(low, ones, preferred_element_type=F32)
+        scale_v[rows, :] = lax.rsqrt(summed * (1.0 / D) + norm_floor)
         return carry
 
-    lax.fori_loop(0, ROWS // 128, factor, 0)
+    lax.fori_loop(0, ROWS // 256, factor, 0)
 
     near = y // 2
 
@@ -308,7 +308,7 @@
 
     def remote_partial(dz, o, r):
         part = pl.ds(pl.multiple_of(512 * r, 512), 512)
-        return remote(pbuf.at[o, dz, part], prx.at[dz, part], prx.at[dz, part], p_send.at[dz, r], p_recv.at[dz, r], partner)
+        return remote(pbuf.at[o, dz, part], prx.at[dz, part], prx.at[dz, part], sent_sem.at[3], p_recv.at[dz, r], partner)
 
     def product(dz, o):
         t = pair_of(dz, o)
@@ -328,20 +328,20 @@
 
     def ring(sign):
         side = 0 if sign == 1 else 1
-        q, k, peer = side, 5 * side, to_x(sign)
+        q, k, peer = side, 6 * side, to_x(sign)
         chunk = lambda ref, base, j: ref.at[pl.ds(base + 256 * j, 256)]
 
         def first(src, j):
             got = chunk(fwd.at[side], 0, j)
-            return remote(chunk(src, 512 * q, j), got, got, r_send.at[k + j], r_recv.at[k + j], peer)
+            return remote(chunk(src, 512 * q, j), got, got, sent_sem.at[4], r_recv.at[k + j], peer)
 
         def second(j):
             got = chunk(fin.at[side], 512 * q, j)
-            return remote(chunk(qf.at[side], 0, j), got, got, r_send.at[k + 2 + j], r_recv.at[k + 2 + j], peer)
-
-        def direct(src):
-            rows = pl.ds(512 * (1 - q), 512)
-            return remote(src.at[rows], fin.at[side, rows], fin.at[side, rows], r_send.at[k + 4], r_recv.at[k + 4], peer)
+            return remote(chunk(qf.at[side], 0, j), got, got, sent_sem.at[4], r_recv.at[k + 2 + j], peer)
+
+        def direct(src, j):
+            got = chunk(fin.at[side], 512 * (1 - q), j)
+            return remote(chunk(src, 512 * (1 - q), j), got, got, sent_sem.at[4], r_recv.at[k + 4 + j], peer)
 
         return first, second, direct
 
@@ -364,7 +364,19 @@
 
                 @pl.when(ahead(dz) == d)
                 def _():
-                    RING[-sign][2](mine)[0]().start()
+                    RING[-sign][2](mine, 0)[0]().start()
+                    if not later(dz, o):
+                        RING[-sign][2](mine, 1)[0]().start()
+
+    later = lambda dz, o: o == 1 and dz in (1, 3)
+
+    def direct_rest(dz, o):
+        @pl.when(core_of(o) == c)
+        def _():
+            for sign, d in ((1, 1), (-1, 3)):
+                @pl.when(ahead(dz) == d)
+                def _():
+                    RING[sign][2](pbuf.at[o, dz], 1)[0]().start()
 
     def forward(dz, o):
         @pl.when(core_of(o) == c)
@@ -386,11 +398,11 @@
     e3b(DN)
     e4a(DN)
     product(1, 0)
-    forward(0, 0)
+    e3c(DN)
     product(3, 0)
-    e3c(DN)
     reduce_pair(1, 0)
     reduce_pair(3, 0)
+    forward(0, 0)
     e4c(DN)
     own_far(DN)
     product(2, 0)
@@ -403,14 +415,16 @@
     product(1, 1)
     reduce_pair(0, 1)
     product(3, 1)
+    forward(3, 0)
     reduce_pair(1, 1)
+    forward(1, 0)
+    reduce_pair(3, 1)
     other_far(DN)
     product(2, 1)
-    forward(3, 0)
-    forward(1, 0)
-    reduce_pair(3, 1)
     forward(2, 0)
     reduce_pair(2, 1)
+    direct_rest(1, 1)
+    direct_rest(3, 1)
     forward(0, 1)
     forward(1, 1)
     forward(3, 1)
@@ -421,7 +435,8 @@
     for sign in (1, -1):
         RING[sign][1](0)[1]().wait_recv()
         RING[sign][1](1)[1]().wait_recv()
-        RING[sign][2](pbuf.at[0, 0])[1]().wait_recv()
+        RING[sign][2](pbuf.at[0, 0], 0)[1]().wait_recv()
+        RING[sign][2](pbuf.at[0, 0], 1)[1]().wait_recv()
 
     def last(m, carry):
         rows = pl.ds(pl.multiple_of(m * TILE, TILE), TILE)
@@ -431,24 +446,17 @@
 
     lax.fori_loop(0, ROWS // TILE, last, 0)
 
-    for send in sends:
-        send.wait_send()
-    for dz in range(4):
-        for r in (0, 1):
-            remote_partial(dz, 0, r)[0]().wait_send()
-    for sign in (1, -1):
-        for j in (0, 1):
-            RING[sign][0](pbuf.at[0, 0], j)[0]().wait_send()
-            RING[sign][1](j)[0]().wait_send()
-        RING[sign][2](pbuf.at[0, 0])[0]().wait_send()
+    for k, ref in enumerate((up_v.at[:, pl.ds(0, 1920)], dn_v.at[pl.ds(0, 15)], tok_v.at[pl.ds(0, 7)], prx, pbuf.at[0, pl.ds(0, 3)])):
+        pltpu.make_async_copy(ref, ref, sent_sem.at[k]).wait()
 
 
 def put_out(up_v, dn_v, out_v, up_out, dn_out, out, sem):
-    copies = [pltpu.make_async_copy(out_v, out, sem.at[18])]
-    for h in (0, 1):
-        copies.append(pltpu.make_async_copy(up_v.at[h], up_out.at[:, pl.ds(512 * h, 512)], sem.at[h]))
+    copies = [pltpu.make_async_copy(out_v, out, sem.at[32])]
     for f in range(16):
-        copies.append(pltpu.make_async_copy(dn_v.at[f], dn_out.at[:, pl.ds(128 * f, 128)], sem.at[2 + f]))
+        copies.append(pltpu.make_async_copy(dn_v.at[f], dn_out.at[:, pl.ds(128 * f, 128)], sem.at[f]))
+    for k in range(16):
+        rows, h = pl.ds(256 * (k // 2), 256), k % 2
+        copies.append(pltpu.make_async_copy(up_v.at[h, rows], up_out.at[rows, pl.ds(512 * h, 512)], sem.at[16 + k]))
     for copy in copies:
         copy.start()
     for copy in copies:
@@ -482,14 +490,11 @@
             pltpu.VMEM((2, 512, 256), BF),
             pltpu.VMEM((2, ROWS, 256), BF),
             pltpu.SemaphoreType.DMA((4,)),
-            pltpu.SemaphoreType.DMA((2, 2, 22)),
+            pltpu.SemaphoreType.DMA((5,)),
             pltpu.SemaphoreType.DMA((2, 2, 22)),
             pltpu.SemaphoreType.DMA((11,)),
-            pltpu.SemaphoreType.DMA((11,)),
             pltpu.SemaphoreType.DMA((4, 2)),
-            pltpu.SemaphoreType.DMA((4, 2)),
-            pltpu.SemaphoreType.DMA((10,)),
-            pltpu.SemaphoreType.DMA((10,)),
+            pltpu.SemaphoreType.DMA((12,)),
         ],
         compiler_params=pltpu.CompilerParams(collective_id=0, has_side_effects=True, vmem_limit_bytes=40 << 20),
     )(in_hbm(tokens), in_hbm(norm_gain.reshape(1, 128)), in_hbm(up_master), in_hbm(down_master))
@@ -503,7 +508,7 @@
         ),
         in_specs=[vmem] * 3,
         out_specs=(anywhere,) * 3,
-        scratch_shapes=[pltpu.SemaphoreType.DMA((19,))],
+        scratch_shapes=[pltpu.SemaphoreType.DMA((33,))],
         compiler_params=pltpu.CompilerParams(vmem_limit_bytes=16 << 20),
     )(*held)
 

time: 74.1 us -> 70.6 us (0.953)
  Pallas kernels: 73.4 us -> 69.9 us
    pallas_call x1, Pallas kernels: 69.8 us -> 66.1 us  [on_device(): pl.pallas_call(kernel, name='gather_mlp', out_shape=(pltpu.VMEM((2, D, 51...]
where the time goes in v3:
time: 70.6 us; the launch traced here: 70.5 us
  Pallas kernels  69.9 us (99%)
    pallas_call x1, Pallas kernels, on_device(): pl.pallas_call(kernel, name='gather_mlp', out_shape=(pltpu.VMEM((2, D, 51...  66.1 us
    pallas_call x1, Pallas kernels, on_device(): pl.pallas_call(put_out, name='put_out', out_shape=(jax.ShapeDtypeStruct((...  3.71 us

profile of v3, /device:TPU:5, one launch (start us, length us, event | category | flops | bytes accessed | tf_op | source)
XLA Modules:
  0.0 70.5 jit_solution(9695988480079394530)
XLA Ops:
  0.6 66.1 %gather_mlp.1 = (bf16[2,2048,512]{2,1,0:T(8,128)(2,1)S(1)}, bf16[16,1024,128]{2,1,0:T(8,128)(2,1)S(1)}, bf16[1024,256]{1,0:T(8,128)(2,1)S(1)}) custom-call(bf16[1024,256]{1,0:T(8,128)(2,1)} %tok_in.1, f32[1,128]{1,0:T(1,128)} %bitcast.1, f32[128,1024]{1,0:T(8,128)} %up_in.1, f32[128,1024]{1,0:T(8,128)} %dn_in.1), custom_call_target="tpu_custom_call" | custom-call | tf_op jit(solution)/shard_map/gather_mlp/pallas_call | solution.py:469
  66.8 3.7 %put_out.1 = (bf16[2048,1024]{1,0:T(8,128)(2,1)}, bf16[1024,2048]{1,0:T(8,128)(2,1)}, bf16[1024,256]{1,0:T(8,128)(2,1)}) custom-call(bf16[2,2048,512]{2,1,0:T(8,128)(2,1)S(1)} %get-tuple-element.6.up_v, bf16[16,1024,128]{2,1,0:T(8,128)(2,1)S(1)} %get-tuple-element.7.dn_v, bf16[1024,256]{1,0:T(8,128)(2,1)S(1)} %get-tuple-element.8.out_v), custom_call_target="tpu_custom_call" | custom-call | tf_op jit(solution)/shard_map/put_out/pallas_call | solution.py:501

commit v4 on v3

--- a/solution.py
+++ b/solution.py
@@ -13,6 +13,12 @@
 ROWS = 1024
 TILE = 512
 UP, DN = 0, 1
+GROUPS = (
+    [(0, j, "G", s) for j in (0, "+") for s in (1, -1)],
+    [(1, 0, "G", s) for s in ("+", "-")],
+    [(0, 2, "T", 1, 1), (0, 2, "T", -1, 0)] + [(1, j, "G", s) for j in (1, -1) for s in ("+", "-")],
+    [(0, j, "G", s) for j in ("-", 2) for s in (1, -1)] + [(1, 2, "T", "-", 0), (1, 2, "G", "+"), (1, 2, "G", "-")],
+)
 
 
 def kernel(
@@ -35,8 +41,8 @@
         pltpu.make_async_copy(tok_in, tok_v.at[tp], in_sem.at[2]),
         pltpu.make_async_copy(dn_in, dn32, in_sem.at[3]),
     ]
-    for load in loads:
-        load.start()
+    loads[0].start()
+    loads[1].start()
     barrier = pltpu.get_barrier_semaphore()
     for peer in (to_y(1), to_y(-1), to_z(1), to_z(-1), to_x(1), to_x(-1), partner):
         pl.semaphore_signal(barrier, inc=1, device_id=peer, device_id_type=MESH)
@@ -61,13 +67,15 @@
             at, n = 512 * h + (0 if q is None else 256 * q), 512 if q is None else 256
             return dn_v.at[f, pl.ds(at, n)]
 
-        tables = ({}, {})
+        tables, single = ({}, {}), [len(GROUPS)]
 
         def add(h, name, sent, side, landed):
-            k = len(tables[h])
+            group = [g for g, names in enumerate(GROUPS) if (h, *name) in names]
+            k = group[0] if group else single[0]
+            single[0] += not group
             peer = to_y(y_at[side]) if side in ("+", "-") else to_z(side)
             src, got = piece(h, *sent), piece(h, *landed)
-            tables[h][name] = remote(src, src, got, sent_sem.at[w], w_recv.at[w, h, k], peer)
+            tables[h][name] = remote(src, src, got, sent_sem.at[w], w_recv.at[w, k], peer)
 
         for s, other, q in (("+", "-", 1), ("-", "+", 0)):
             add(0, ("S", s), (0, 0, None), s, (s, 0, None))
@@ -95,6 +103,14 @@
         for name in names:
             W[w][h][name][1]().wait_recv()
 
+    def take_group(w, g):
+        n = len(GROUPS[g])
+        if w == UP:
+            ref = up_v.at[0, pl.ds(0, 64 * n)]
+        else:
+            ref = dn_v.at[pl.ds(0, n), pl.ds(0, 256)]
+        pltpu.make_async_copy(ref, ref, w_recv.at[w, g]).wait()
+
     def put(w, h, *names):
         for name in names:
             go(W[w][h][name])
@@ -141,14 +157,14 @@
             take(w, 0, ("F", s))
             put(w, 0, (2, "T", 1, q), (2, "T", -1, q))
 
-    def e4a(w):
-        for jz in (-1, 1):
+    def e4a(w, sides=(-1, 1)):
+        for jz in sides:
             for s, other in (("+", "-"), ("-", "+")):
                 take(w, 1, (jz, "T", s))
                 put(w, 1, (jz, "G", other))
 
     def own_far(w):
-        take(w, 0, (0, "G", 1), (0, "G", -1), ("+", "G", 1), ("+", "G", -1))
+        take_group(w, 0)
         take(w, 1, (2, "T", "+", 0))
         put(w, 1, (2, "G", "-"))
         take(w, 1, (2, "T", "+", 1))
@@ -168,15 +184,13 @@
             put(w, 0, (2, "G", s))
 
     def other_near(w):
-        take(w, 1, (0, "G", "+"), (0, "G", "-"))
+        take_group(w, 1)
 
     def other_side(w):
-        take(w, 0, (2, "T", 1, 1), (2, "T", -1, 0))
-        take(w, 1, *[(jz, "G", s) for jz in (1, -1) for s in ("+", "-")])
+        take_group(w, 2)
 
     def other_far(w):
-        take(w, 0, ("-", "G", 1), ("-", "G", -1), (2, "G", 1), (2, "G", -1))
-        take(w, 1, (2, "T", "-", 0), (2, "G", "+"), (2, "G", "-"))
+        take_group(w, 3)
 
     def rows_of(t, half):
         return tok_v.at[t] if half is None else tok_v.at[t, pl.ds(512 * half, 512)]
@@ -185,7 +199,7 @@
     T = {}
 
     def token_copy(name, d_sent, half, peer, d_landed, core_landed):
-        k = len(T)
+        k = min(len(T), 6)
         sent, got = rows_of(block(d_sent, c), half), rows_of(block(d_landed, core_landed), half)
         T[name] = remote(sent, sent, got, sent_sem.at[2], t_recv.at[k], peer)
 
@@ -201,17 +215,19 @@
     token_copy(("D", 2, 1), 2, 1, partner, 2, 1 - c)
 
     loads[0].wait()
+    loads[2].start()
+    loads[3].start()
     loads[1].wait()
     gain = jnp.transpose(jnp.broadcast_to(gain_v[...], (128, 128)))
     for h in (0, 1):
         for k in range(4):
             cols = slice(512 * h + 128 * k, 512 * h + 128 * k + 128)
             up_v[h, pl.ds(pl.multiple_of(fs * 128, 128), 128), 128 * k : 128 * k + 128] = (gain * up32[:, cols]).astype(BF)
-    loads[2].wait()
     pl.semaphore_wait(barrier, 7)
 
     e0y(UP)
     e0z(UP)
+    loads[2].wait()
     go(T["X+", 0]), go(T["X-", 1]), go(T["X+", 1]), go(T["X-", 0])
     go(T["D", 0])
 
@@ -243,8 +259,7 @@
     e0y(DN)
     e4d(UP)
     e0z(DN)
-    for name in (("D", 0), ("D", -1), ("D", 1), ("D", 2, 0), ("D", 2, 1)):
-        T[name][1]().wait_recv()
+    pltpu.make_async_copy(tok_v.at[pl.ds(0, 4)], tok_v.at[pl.ds(0, 4)], t_recv.at[6]).wait()
 
     ones = jnp.ones((128, 128), BF)
 
@@ -328,7 +343,7 @@
 
     def ring(sign):
         side = 0 if sign == 1 else 1
-        q, k, peer = side, 6 * side, to_x(sign)
+        q, k, peer = side, 2 * side, to_x(sign)
         chunk = lambda ref, base, j: ref.at[pl.ds(base + 256 * j, 256)]
 
         def first(src, j):
@@ -337,11 +352,11 @@
 
         def second(j):
             got = chunk(fin.at[side], 512 * q, j)
-            return remote(chunk(qf.at[side], 0, j), got, got, sent_sem.at[4], r_recv.at[k + 2 + j], peer)
+            return remote(chunk(qf.at[side], 0, j), got, got, sent_sem.at[4], r_recv.at[4], peer)
 
         def direct(src, j):
             got = chunk(fin.at[side], 512 * (1 - q), j)
-            return remote(chunk(src, 512 * (1 - q), j), got, got, sent_sem.at[4], r_recv.at[k + 4 + j], peer)
+            return remote(chunk(src, 512 * (1 - q), j), got, got, sent_sem.at[4], r_recv.at[4], peer)
 
         return first, second, direct
 
@@ -395,29 +410,30 @@
     product(0, 0)
     e3a(DN)
     reduce_pair(0, 0)
+    e4a(DN, (-1,))
+    product(3, 0)
     e3b(DN)
-    e4a(DN)
+    reduce_pair(3, 0)
+    e4a(DN, (1,))
     product(1, 0)
     e3c(DN)
-    product(3, 0)
     reduce_pair(1, 0)
-    reduce_pair(3, 0)
     forward(0, 0)
-    e4c(DN)
     own_far(DN)
     product(2, 0)
+    e4c(DN)
+    reduce_pair(2, 0)
     e4b(DN)
+    forward(3, 0)
     other_near(DN)
     product(0, 1)
-    reduce_pair(2, 0)
     e4d(DN)
     other_side(DN)
     product(1, 1)
     reduce_pair(0, 1)
     product(3, 1)
-    forward(3, 0)
+    forward(1, 0)
     reduce_pair(1, 1)
-    forward(1, 0)
     reduce_pair(3, 1)
     other_far(DN)
     product(2, 1)
@@ -432,11 +448,7 @@
 
     mine = mod4(x - z)
     o_mine = jnp.where(near == c, 0, 1)
-    for sign in (1, -1):
-        RING[sign][1](0)[1]().wait_recv()
-        RING[sign][1](1)[1]().wait_recv()
-        RING[sign][2](pbuf.at[0, 0], 0)[1]().wait_recv()
-        RING[sign][2](pbuf.at[0, 0], 1)[1]().wait_recv()
+    pltpu.make_async_copy(fin, fin, r_recv.at[4]).wait()
 
     def last(m, carry):
         rows = pl.ds(pl.multiple_of(m * TILE, TILE), TILE)
@@ -491,10 +503,10 @@
             pltpu.VMEM((2, ROWS, 256), BF),
             pltpu.SemaphoreType.DMA((4,)),
             pltpu.SemaphoreType.DMA((5,)),
-            pltpu.SemaphoreType.DMA((2, 2, 22)),
-            pltpu.SemaphoreType.DMA((11,)),
+            pltpu.SemaphoreType.DMA((2, 29)),
+            pltpu.SemaphoreType.DMA((7,)),
             pltpu.SemaphoreType.DMA((4, 2)),
-            pltpu.SemaphoreType.DMA((12,)),
+            pltpu.SemaphoreType.DMA((5,)),
         ],
         compiler_params=pltpu.CompilerParams(collective_id=0, has_side_effects=True, vmem_limit_bytes=40 << 20),
     )(in_hbm(tokens), in_hbm(norm_gain.reshape(1, 128)), in_hbm(up_master), in_hbm(down_master))

time: 70.6 us -> 70.1 us (level)
  no operation moved by 1% of the time
where the time goes in v4:
time: 70.1 us; the launch traced here: 70 us
  Pallas kernels  69.3 us (99%)
    pallas_call x1, Pallas kernels, on_device(): pl.pallas_call(kernel, name='gather_mlp', out_shape=(pltpu.VMEM((2, D, 51...  65.6 us
    pallas_call x1, Pallas kernels, on_device(): pl.pallas_call(put_out, name='put_out', out_shape=(jax.ShapeDtypeStruct((...  3.71 us

profile of v4, /device:TPU:5, one launch (start us, length us, event | category | flops | bytes accessed | tf_op | source)
XLA Modules:
  0.0 70.0 jit_solution(16446154435113848187)
XLA Ops:
  0.6 65.6 %gather_mlp.1 = (bf16[2,2048,512]{2,1,0:T(8,128)(2,1)S(1)}, bf16[16,1024,128]{2,1,0:T(8,128)(2,1)S(1)}, bf16[1024,256]{1,0:T(8,128)(2,1)S(1)}) custom-call(bf16[1024,256]{1,0:T(8,128)(2,1)} %tok_in.1, f32[1,128]{1,0:T(1,128)} %bitcast.1, f32[128,1024]{1,0:T(8,128)} %up_in.1, f32[128,1024]{1,0:T(8,128)} %dn_in.1), custom_call_target="tpu_custom_call" | custom-call | tf_op jit(solution)/shard_map/gather_mlp/pallas_call | solution.py:481
  66.2 3.7 %put_out.1 = (bf16[2048,1024]{1,0:T(8,128)(2,1)}, bf16[1024,2048]{1,0:T(8,128)(2,1)}, bf16[1024,256]{1,0:T(8,128)(2,1)}) custom-call(bf16[2,2048,512]{2,1,0:T(8,128)(2,1)S(1)} %get-tuple-element.6.up_v, bf16[16,1024,128]{2,1,0:T(8,128)(2,1)S(1)} %get-tuple-element.7.dn_v, bf16[1024,256]{1,0:T(8,128)(2,1)S(1)} %get-tuple-element.8.out_v), custom_call_target="tpu_custom_call" | custom-call | tf_op jit(solution)/shard_map/put_out/pallas_call | solution.py:513

commit v5 on v4

--- a/solution.py
+++ b/solution.py
@@ -23,8 +23,8 @@
 
 def kernel(
     tok_in, gain_in, up_in, dn_in,
-    up_v, dn_v, out_v,
-    up32, dn32, gain_v, tok_v, scale_v, acc, hid, pbuf, prx, fwd, qf, fin,
+    up_v, dn_v, own_v, fin,
+    up32, dn32, gain_v, tok_v, scale_v, acc, hid, pbuf, prx, fwd, qf,
     in_sem, sent_sem, w_recv, t_recv, p_recv, r_recv,
 ):
     fs, tp = lax.axis_index("fs"), lax.axis_index("tp")
@@ -371,6 +371,10 @@
                 remote_partial(dz, o, r)[1]().wait_recv()
                 rows = pl.ds(512 * r, 512)
                 pbuf[o, dz, rows, :] = (pbuf[o, dz, rows, :].astype(F32) + prx[dz, rows, :].astype(F32)).astype(BF)
+
+                @pl.when(ahead(dz) == 0)
+                def _():
+                    own_v[rows, :] = pbuf[o, dz, rows, :]
 
                 @pl.when(ahead(dz) == 2)
                 def _():
@@ -446,24 +450,14 @@
     forward(3, 1)
     forward(2, 1)
 
-    mine = mod4(x - z)
-    o_mine = jnp.where(near == c, 0, 1)
     pltpu.make_async_copy(fin, fin, r_recv.at[4]).wait()
-
-    def last(m, carry):
-        rows = pl.ds(pl.multiple_of(m * TILE, TILE), TILE)
-        total = pbuf[o_mine, mine, rows, :].astype(F32) + fin[0, rows, :].astype(F32) + fin[1, rows, :].astype(F32)
-        out_v[rows, :] = total.astype(BF)
-        return carry
-
-    lax.fori_loop(0, ROWS // TILE, last, 0)
 
     for k, ref in enumerate((up_v.at[:, pl.ds(0, 1920)], dn_v.at[pl.ds(0, 15)], tok_v.at[pl.ds(0, 7)], prx, pbuf.at[0, pl.ds(0, 3)])):
         pltpu.make_async_copy(ref, ref, sent_sem.at[k]).wait()
 
 
-def put_out(up_v, dn_v, out_v, up_out, dn_out, out, sem):
-    copies = [pltpu.make_async_copy(out_v, out, sem.at[32])]
+def put_out(up_v, dn_v, own_v, fin, up_out, dn_out, out, out_v, sem):
+    copies = []
     for f in range(16):
         copies.append(pltpu.make_async_copy(dn_v.at[f], dn_out.at[:, pl.ds(128 * f, 128)], sem.at[f]))
     for k in range(16):
@@ -471,6 +465,12 @@
         copies.append(pltpu.make_async_copy(up_v.at[h, rows], up_out.at[rows, pl.ds(512 * h, 512)], sem.at[16 + k]))
     for copy in copies:
         copy.start()
+    for m in range(ROWS // 256):
+        rows = pl.ds(256 * m, 256)
+        total = own_v[rows, :].astype(F32) + fin[0, rows, :].astype(F32) + fin[1, rows, :].astype(F32)
+        out_v[rows, :] = total.astype(BF)
+    copies.append(pltpu.make_async_copy(out_v, out, sem.at[32]))
+    copies[-1].start()
     for copy in copies:
         copy.wait()
 
@@ -485,9 +485,10 @@
             pltpu.VMEM((2, D, 512), BF),
             pltpu.VMEM((16, 1024, 128), BF),
             pltpu.VMEM((ROWS, 256), BF),
+            pltpu.VMEM((2, ROWS, 256), BF),
         ),
         in_specs=[anywhere] * 4,
-        out_specs=(vmem, vmem, vmem),
+        out_specs=(vmem,) * 4,
         scratch_shapes=[
             pltpu.VMEM((128, 1024), F32),
             pltpu.VMEM((128, 1024), F32),
@@ -500,7 +501,6 @@
             pltpu.VMEM((4, ROWS, 256), BF),
             pltpu.VMEM((2, 512, 256), BF),
             pltpu.VMEM((2, 512, 256), BF),
-            pltpu.VMEM((2, ROWS, 256), BF),
             pltpu.SemaphoreType.DMA((4,)),
             pltpu.SemaphoreType.DMA((5,)),
             pltpu.SemaphoreType.DMA((2, 29)),
@@ -518,9 +518,9 @@
             jax.ShapeDtypeStruct((1024, D), BF),
             jax.ShapeDtypeStruct((ROWS, 256), BF),
         ),
-        in_specs=[vmem] * 3,
+        in_specs=[vmem] * 4,
         out_specs=(anywhere,) * 3,
-        scratch_shapes=[pltpu.SemaphoreType.DMA((33,))],
+        scratch_shapes=[pltpu.VMEM((ROWS, 256), BF), pltpu.SemaphoreType.DMA((33,))],
         compiler_params=pltpu.CompilerParams(vmem_limit_bytes=16 << 20),
     )(*held)
 

time: 70.1 us -> 70 us (level)
  no operation moved by 1% of the time
where the time goes in v5:
time: 70 us; the launch traced here: 69.8 us
  Pallas kernels  69.1 us (99%)
    pallas_call x1, Pallas kernels, on_device(): pl.pallas_call(kernel, name='gather_mlp', out_shape=(pltpu.VMEM((2, D, 51...  65.4 us
    pallas_call x1, Pallas kernels, on_device(): pl.pallas_call(put_out, name='put_out', out_shape=(jax.ShapeDtypeStruct((...  3.72 us

profile of v5, /device:TPU:5, one launch (start us, length us, event | category | flops | bytes accessed | tf_op | source)
XLA Modules:
  0.0 69.8 jit_solution(16658060565903741236)
XLA Ops:
  0.6 65.4 %gather_mlp.1 = (bf16[2,2048,512]{2,1,0:T(8,128)(2,1)S(1)}, bf16[16,1024,128]{2,1,0:T(8,128)(2,1)S(1)}, bf16[1024,256]{1,0:T(8,128)(2,1)S(1)}, bf16[2,1024,256]{2,1,0:T(8,128)(2,1)S(1)}) custom-call(bf16[1024,256]{1,0:T(8,128)(2,1)} %tok_in.1, f32[1,128]{1,0:T(1,128)} %bitcast.1, f32[128,1024]{1,0:T(8,128)} %up_in.1, f32[128,1024]{1,0:T(8,128)} %dn_in.1), custom_call_target="tpu_custom_call" | custom-call | tf_op jit(solution)/shard_map/gather_mlp/pallas_call | solution.py:481
  66.1 3.7 %put_out.1 = (bf16[2048,1024]{1,0:T(8,128)(2,1)}, bf16[1024,2048]{1,0:T(8,128)(2,1)}, bf16[1024,256]{1,0:T(8,128)(2,1)}) custom-call(bf16[2,2048,512]{2,1,0:T(8,128)(2,1)S(1)} %get-tuple-element.7.up_v, bf16[16,1024,128]{2,1,0:T(8,128)(2,1)S(1)} %get-tuple-element.8.dn_v, bf16[1024,256]{1,0:T(8,128)(2,1)S(1)} %get-tuple-element.9.own_v, ...), custom_call_target="tpu_custom_call" | custom-call | tf_op jit(solution)/shard_map/put_out/pallas_call | solution.py:513

commit v6 on v4

--- a/solution.py
+++ b/solution.py
@@ -408,17 +408,17 @@
                         RING[sign][1](j)[0]().start()
 
     product(0, 0)
+    reduce_pair(0, 0)
     e3a(DN)
-    reduce_pair(0, 0)
     e4a(DN, (-1,))
     product(3, 0)
     e3b(DN)
     reduce_pair(3, 0)
+    forward(0, 0)
     e4a(DN, (1,))
     product(1, 0)
     e3c(DN)
     reduce_pair(1, 0)
-    forward(0, 0)
     own_far(DN)
     product(2, 0)
     e4c(DN)

time: 70.1 us -> 70.1 us (level)
  no operation moved by 1% of the time
where the time goes in v6:
time: 70.1 us; the launch traced here: 70 us
  Pallas kernels  69.3 us (99%)
    pallas_call x1, Pallas kernels, on_device(): pl.pallas_call(kernel, name='gather_mlp', out_shape=(pltpu.VMEM((2, D, 51...  65.6 us
    pallas_call x1, Pallas kernels, on_device(): pl.pallas_call(put_out, name='put_out', out_shape=(jax.ShapeDtypeStruct((...  3.71 us

profile of v6, /device:TPU:5, one launch (start us, length us, event | category | flops | bytes accessed | tf_op | source)
XLA Modules:
  0.0 70.0 jit_solution(16354945810409655369)
XLA Ops:
  0.6 65.6 %gather_mlp.1 = (bf16[2,2048,512]{2,1,0:T(8,128)(2,1)S(1)}, bf16[16,1024,128]{2,1,0:T(8,128)(2,1)S(1)}, bf16[1024,256]{1,0:T(8,128)(2,1)S(1)}) custom-call(bf16[1024,256]{1,0:T(8,128)(2,1)} %tok_in.1, f32[1,128]{1,0:T(1,128)} %bitcast.1, f32[128,1024]{1,0:T(8,128)} %up_in.1, f32[128,1024]{1,0:T(8,128)} %dn_in.1), custom_call_target="tpu_custom_call" | custom-call | tf_op jit(solution)/shard_map/gather_mlp/pallas_call | solution.py:481
  66.2 3.7 %put_out.1 = (bf16[2048,1024]{1,0:T(8,128)(2,1)}, bf16[1024,2048]{1,0:T(8,128)(2,1)}, bf16[1024,256]{1,0:T(8,128)(2,1)}) custom-call(bf16[2,2048,512]{2,1,0:T(8,128)(2,1)S(1)} %get-tuple-element.6.up_v, bf16[16,1024,128]{2,1,0:T(8,128)(2,1)S(1)} %get-tuple-element.7.dn_v, bf16[1024,256]{1,0:T(8,128)(2,1)S(1)} %get-tuple-element.8.out_v), custom_call_target="tpu_custom_call" | custom-call | tf_op jit(solution)/shard_map/put_out/pallas_call | solution.py:513
